TPU v7x, 512 devices: a 4x2x32 block of a 4x8x32 slice. The times are simulated.
512 devices in a mesh: grp: 2 (over y), kv: 32 (over z), tp: 8 (over x, core).
Axes of the slice: x: 4, y: 2, z: 32, core: 2. Of those that a mesh axis runs over, the one named last changes fastest.
The devices are a block of a 4x8x32 slice.
Arguments:
- tokens: bfloat16 [256, 4096], P('grp', 'kv'), parts along dimension 0, may hold values from -40 to 40
- lengths: int32 [256], P(('grp', 'kv')), parts along dimension 0, may hold values from 1 to 6, 320 in all
- conv_state_x: bfloat16 [256, 3, 4096], P(('grp', 'kv'), None, 'tp'), parts along dimension 0, may hold values from -6 to 6
- conv_state_bc: bfloat16 [256, 3, 2, 1024], P(('grp', 'kv'), None, None, 'tp'), parts along dimension 0, may hold values from -6 to 6
- ssm_state: float32 [256, 64, 64, 128], P(('grp', 'kv'), 'tp'), parts along dimension 0, may hold values from -0.6 to 0.6
- norm_gain: bfloat16 [4096], P('kv'), may hold values from 0.099609375 to 1.8984375
- w_gate: bfloat16 [4096, 4096], P('kv', 'tp'), may hold values from -0.09375 to 0.09375
- w_value: bfloat16 [4096, 4096], P('kv', 'tp'), may hold values from -0.09375 to 0.09375
- w_key: bfloat16 [4096, 1024], P('kv', 'tp'), may hold values from -0.09375 to 0.09375
- w_query: bfloat16 [4096, 1024], P('kv', 'tp'), may hold values from -0.09375 to 0.09375
- w_step: bfloat16 [4096, 64], P('kv', 'tp'), may hold values from -0.09375 to 0.09375
- step_bias: float32 [64], P('tp'), may hold values from -2 to 0
- decay_log: float32 [64], P('tp'), may hold values from -2 to 1
- conv_x: bfloat16 [4, 4096], P(None, 'tp'), may hold values from -3 to 3
- conv_bc: bfloat16 [4, 2, 1024], P(None, None, 'tp'), may hold values from -3 to 3
- inner_gain: bfloat16 [4096], P('tp'), may hold values from 0.099609375 to 1.8984375
- w_out: bfloat16 [4096, 4096], P('tp', 'kv'), may hold values from -0.09375 to 0.09375
- mlp_gain: bfloat16 [4096], P('kv'), may hold values from 0.099609375 to 1.8984375
- w_up: bfloat16 [4096, 16384], P('kv', 'tp'), may hold values from -0.09375 to 0.09375
- w_down: bfloat16 [16384, 4096], P('tp', 'kv'), may hold values from -0.046875 to 0.046875
Outputs:
- layer_out: bfloat16 [256, 4096], P('grp', 'kv'), parts along dimension 0
- next_state: float32 [256, 64, 64, 128], P(('grp', 'kv'), 'tp'), parts along dimension 0
There are 2 independent parts, one for each index of `grp`. A program takes and returns all parts, laid end to end along the dimension named above; an argument that names none is the same for every part. Nothing has to cross between parts.
All inputs are finite; a program needn't handle non-finite values. No bound on the sum of `lengths` on one device may be relied on, other than what follows from the above.
Results may differ from a plain program's by a relative error of at most 0.008.
Values may be sent and summed in bfloat16 or wider, within the bound.
No kernel may reach another device: no remote copies, remote signals or barrier semaphores. Data moves between devices by JAX's collectives and lax.ppermute only.
A program may use at most 64 MiB of HBM per device.

v0:
```python
import jax
import jax.numpy as jnp
from jax import lax
from jax.sharding import PartitionSpec as P

D = 4096
HEAD_DIM = 64
STATE = 128
CONV_WIDTH = 4
INNER = 4096
epsilon = 1e-06


def in_blocks(shard, dim, size):
    before, after = (shard.shape[:dim], shard.shape[dim + 1 :])
    return jnp.moveaxis(shard.reshape(*before, size, -1, *after), dim, 0)


def summed_on_arrival(shard, axis, dim):
    parts = in_blocks(shard, dim, lax.axis_size(axis))
    arrived = lax.all_to_all(parts, axis, split_axis=0, concat_axis=0, tiled=True)
    return arrived.sum(axis=0)


def in_one_piece(arrays, axis, dim, along):
    columns = [a.reshape(*a.shape[:along], -1) for a in arrays]
    both = jnp.concatenate(columns, axis=along)
    filled, at, finished = (summed_on_arrival(both, axis, dim), 0, [])
    for a, column in zip(arrays, columns):
        slab = filled[..., at : at + column.shape[along]]
        finished.append(slab.reshape(*slab.shape[:along], *a.shape[along:]))
        at += column.shape[along]
    return tuple(finished)


def from_everyone(shard, axis):
    copies = jnp.broadcast_to(shard, (lax.axis_size(axis), *shard.shape))
    return lax.all_to_all(copies, axis, split_axis=0, concat_axis=0, tiled=True)


def over_copies(shard, axis):
    return from_everyone(shard, axis).sum(axis=0)


def laid_out(parts, dim):
    shape = list(parts.shape[1:])
    shape[dim] *= parts.shape[0]
    return jnp.moveaxis(parts, 0, dim).reshape(shape)


def gathered_copies(shard, axis, dim):
    parts = from_everyone(shard, axis)
    return laid_out(parts, dim)


def causal_conv(state_rows, newest, conv_weights):
    extended = jnp.concatenate([state_rows, newest[:, None]], axis=1)
    conv_sum = extended[:, 0] * conv_weights[0].astype(jnp.float32)
    for offset in range(1, conv_weights.shape[0]):
        conv_sum = conv_sum + extended[:, offset] * conv_weights[offset].astype(jnp.float32)
    return jax.nn.silu(conv_sum)


def product(left, right):
    return jnp.dot(left, right, preferred_element_type=jnp.float32)


def per_device(
    tokens,
    lengths,
    conv_state_x,
    conv_state_bc,
    ssm_state,
    norm_gain,
    w_gate,
    w_value,
    w_key,
    w_query,
    w_step,
    step_bias,
    decay_log,
    conv_x,
    conv_bc,
    inner_gain,
    w_out,
    mlp_gain,
    w_up,
    w_down,
):
    head_count = w_step.shape[1]
    group_count = w_key.shape[1] // STATE
    per_group = head_count // group_count
    widened = tokens.astype(jnp.float32)
    scaled = (widened * norm_gain.astype(jnp.float32)).astype(jnp.bfloat16)
    gate_raw, value_raw, key_raw, query_raw, step_raw, squares = in_one_piece(
        (
            product(scaled, w_gate),
            product(scaled, w_value),
            product(scaled, w_key),
            product(scaled, w_query),
            product(scaled, w_step),
            jnp.sum(widened * widened, axis=1),
        ),
        "kv",
        0,
        1,
    )
    seq_count = gate_raw.shape[0]
    inverse = lax.rsqrt(squares / D + epsilon)[:, None]
    row_live = (
        jnp.arange(CONV_WIDTH - 1, dtype=jnp.int32)[None, :] >= CONV_WIDTH - 1 - lengths[:, None]
    ).astype(jnp.float32)
    live_x = conv_state_x.astype(jnp.float32) * row_live[:, :, None]
    live_bc = conv_state_bc.astype(jnp.float32) * row_live[:, :, None, None]
    mixed_values = causal_conv(live_x, value_raw * inverse, conv_x).reshape(
        seq_count, head_count, HEAD_DIM
    )
    key_query = causal_conv(
        live_bc, jnp.stack([key_raw * inverse, query_raw * inverse], axis=1), conv_bc
    )
    key_heads = jnp.repeat(
        key_query[:, 0].reshape(seq_count, group_count, STATE), per_group, axis=1
    )
    query_heads = jnp.repeat(
        key_query[:, 1].reshape(seq_count, group_count, STATE), per_group, axis=1
    )
    step_size = jax.nn.softplus(step_raw * inverse + step_bias)
    rate_now = -jnp.exp(decay_log) * step_size
    next_state = (
        ssm_state * jnp.exp(rate_now)[:, :, None, None]
        + (step_size[:, :, None] * mixed_values)[:, :, :, None] * key_heads[:, :, None, :]
    )
    mixer_y = jnp.einsum(
        "bhpn,bhn->bhp", next_state, query_heads, precision=lax.Precision.HIGHEST
    ).reshape(seq_count, head_count * HEAD_DIM)
    gated_rows = mixer_y * jax.nn.silu(gate_raw * inverse)
    gated_low = (gated_rows * inner_gain.astype(jnp.float32)).astype(jnp.bfloat16)
    all_low, all_squares = (
        lax.all_gather(gated_low, "kv", axis=0, tiled=True),
        lax.all_gather(
            jnp.sum(gated_rows * gated_rows, axis=1).astype(jnp.bfloat16), "kv", axis=0, tiled=True
        ).astype(jnp.float32),
    )
    out_sum, gated_total = (
        over_copies(product(all_low, w_out), "tp"),
        over_copies(all_squares, "tp"),
    )
    residual = (widened + out_sum * lax.rsqrt(gated_total / INNER + epsilon)[:, None]).astype(
        jnp.bfloat16
    )
    residual_wide = residual.astype(jnp.float32)
    hidden_low = (residual_wide * mlp_gain.astype(jnp.float32)).astype(jnp.bfloat16)
    row_squares = jnp.sum(residual_wide * residual_wide, axis=1)
    up_share, square_share = in_one_piece((product(hidden_low, w_up), row_squares), "kv", 0, 1)
    share_active = jnp.square(
        jax.nn.relu(up_share * lax.rsqrt(square_share / D + epsilon)[:, None])
    ).astype(jnp.bfloat16)
    activation = gathered_copies(share_active, "kv", 0)
    down_sum = over_copies(product(activation, w_down), "tp")
    layer_out = (residual_wide + down_sum).astype(jnp.bfloat16)
    return (layer_out, next_state)


def solution(mesh):
    return jax.shard_map(
        per_device,
        mesh=mesh,
        in_specs=(
            P("grp", "kv"),
            P(("grp", "kv")),
            P(("grp", "kv"), None, "tp"),
            P(("grp", "kv"), None, None, "tp"),
            P(("grp", "kv"), "tp", None, None),
            P("kv"),
            P("kv", "tp"),
            P("kv", "tp"),
            P("kv", "tp"),
            P("kv", "tp"),
            P("kv", "tp"),
            P("tp"),
            P("tp"),
            P(None, "tp"),
            P(None, None, "tp"),
            P("tp"),
            P("tp", "kv"),
            P("kv"),
            P("kv", "tp"),
            P("tp", "kv"),
        ),
        out_specs=(P("grp", "kv"), P(("grp", "kv"), "tp", None, None)),
        check_vma=False,
    )
```

profile of v0, /device:TPU:33, one launch (start us, length us, event | category | flops | bytes accessed | tf_op | source)
XLA Modules:
  0.0 471.4 jit_solution(15149226765499633924)
XLA Ops:
  0.7 0.7 convert_element_type.73
  1.4 0.9 fusion.1
  2.3 0.3 concatenate.34
  2.5 0.9 fusion.16
  3.4 0.9 fusion.14
  4.3 0.9 fusion.12
  5.2 1.1 fusion.18
  6.3 0.1 concatenate.25
  6.4 0.2 fusion.20
  6.6 0.1 concatenate.24
  6.8 1.2 concatenate.30
  8.0 46.4 %all-to-all-start = ((f32[32,4,1289]{2,1,0:T(4,128)}), f32[32,4,1289]{2,1,0:T(4,128)S(1)}, u32[]{:S(2)}, u32[]{:S(2)}) async-start(f32[32,4,1289]{2,1,0:T(4,128)} %concatenate.30), calls=%async_computation | async-start | bytes 1441792 | tf_op jit(solution)/shard_map/all_to_all | solution.py:21
  54.4 1.3 dynamic-slice
  56.6 79.0 %all-to-all-done = f32[32,4,1289]{2,1,0:T(4,128)S(1)} async-done(((f32[32,4,1289]{2,1,0:T(4,128)}), f32[32,4,1289]{2,1,0:T(4,128)S(1)}, u32[]{:S(2)}, u32[]{:S(2)}) %all-to-all-start) | async-done | bytes 660000 | tf_op jit(solution)/shard_map/all_to_all | solution.py:21
  135.6 0.1 reduce_sum.73
  135.7 0.2 fusion.44
  135.9 0.1 fusion.41
  136.0 0.1 divide_multiply_fusion.1
  136.1 0.1 reshape.98
  136.2 0.1 multiply_exponential_fusion
  136.3 0.4 multiply_add_fusion
  136.8 1.7 fusion.49
  138.5 0.1 reshape.100
  138.6 0.2 multiply_reduce_fusion
  138.8 0.2 dynamic-update-slice
  139.1 39.4 %all-reduce = bf16[128]{0:T(256)(128)(2,1)S(1)} all-reduce(bf16[128]{0:T(256)(128)(2,1)S(1)} %dynamic-update-slice), channel_id=1, replica_groups=mesh['grp'=2,'kv'=32,'tp'=8] {'kv'}, use_global_device_ids=true, to_apply=%add | all-reduce | flops 128 | bytes 512
  178.5 0.6 broadcast_in_dim.9
  179.1 18.6 %all-to-all-start.2 = ((f32[8,1,128]{2,1,0:T(1,128)}), f32[8,1,128]{2,1,0:T(1,128)S(1)}, u32[]{:S(2)}, u32[]{:S(2)}) async-start(f32[8,1,128]{2,1,0:T(1,128)} %broadcast_in_dim.9), calls=%async_computation.2 | async-start | bytes 8192 | tf_op jit(solution)/shard_map/all_to_all | solution.py:38
  197.7 40.2 %all-gather = bf16[32,4,512]{2,1,0:T(4,128)(2,1)S(1)} all-gather(bf16[1,4,512]{2,1,0:T(4,128)(2,1)S(1)} %fusion.30), channel_id=1, replica_groups=mesh['grp'=2,'kv'=32,'tp'=8] {'kv'}, dimensions={0}, use_global_device_ids=true | all-gather | bytes 135168 | tf_op jit(solution)/shard_map/all_gather | solution.py:139
  238.0 0.2 fusion.50
  238.2 0.8 broadcast_in_dim.8
  239.0 18.5 %all-to-all-start.1 = ((f32[8,128,128]{2,1,0:T(8,128)}), f32[8,128,128]{2,1,0:T(8,128)S(1)}, u32[]{:S(2)}, u32[]{:S(2)}) async-start(f32[8,128,128]{2,1,0:T(8,128)} %broadcast_in_dim.8), calls=%async_computation.1 | async-start | bytes 1048576 | tf_op jit(solution)/shard_map/all_to_all | solution.py:38
  257.6 9.3 %all-to-all-done.1 = f32[8,128,128]{2,1,0:T(8,128)S(1)} async-done(((f32[8,128,128]{2,1,0:T(8,128)}), f32[8,128,128]{2,1,0:T(8,128)S(1)}, u32[]{:S(2)}, u32[]{:S(2)}) %all-to-all-start.1) | async-done | bytes 524320 | tf_op jit(solution)/shard_map/all_to_all | solution.py:38
  266.9 0.2 fusion.4
  267.1 0.3 concatenate.35
  267.4 0.3 fusion.6
  267.7 0.3 concatenate.31
  268.0 0.2 pad_maximum_fusion
  268.2 120.2 %all_to_all.31 = f32[32,4,2049]{2,1,0:T(4,128)S(1)} all-to-all(f32[32,4,2049]{2,1,0:T(4,128)S(1)} %pad_maximum_fusion), channel_id=1, replica_groups=mesh['grp'=2,'kv'=32,'tp'=8] {'kv'}, dimensions={0} | all-to-all | bytes 2098176 | tf_op jit(solution)/shard_map/all_to_all | solution.py:21
  388.4 0.2 reduce_sum.78
  388.6 0.1 fusion.39
  388.7 0.1 fusion.10
  388.8 0.2 broadcast_in_dim.10
  389.1 64.8 %all_to_all.32 = bf16[32,4,2048]{2,1,0:T(4,128)(2,1)S(1)} all-to-all(bf16[32,4,2048]{2,1,0:T(4,128)(2,1)S(1)} %broadcast_in_dim.10), channel_id=1, replica_groups=mesh['grp'=2,'kv'=32,'tp'=8] {'kv'}, dimensions={0} | all-to-all | bytes 1048576 | tf_op jit(solution)/shard_map/all_to_all | solution.py:38
  453.8 0.1 reshape.101
  454.0 0.3 fusion.51
  454.3 16.5 %all_to_all.33 = f32[8,128,128]{2,1,0:T(8,128)S(1)} all-to-all(f32[8,128,128]{2,1,0:T(8,128)S(1)} %broadcast_in_dim.11), channel_id=1, replica_groups=mesh['grp'=2,'kv'=32,'tp'=8] {'tp'}, dimensions={0} | all-to-all | bytes 1048576 | tf_op jit(solution)/shard_map/all_to_all | solution.py:38
  470.8 0.6 fusion.5
  (54 shorter events, 0.5 us)
Async XLA Ops:
  0.6 266.7 %copy-start = (bf16[128,2048]{1,0:T(8,128)(2,1)S(1)}, bf16[128,2048]{1,0:T(8,128)(2,1)}, u32[]{:S(2)}) copy-start(bf16[128,2048]{1,0:T(8,128)(2,1)} %param.38) | copy-start | bytes 1572868
  0.6 5.8 %copy-start.2 = (bf16[128,128]{1,0:T(8,128)(2,1)S(1)}, bf16[128,128]{1,0:T(8,128)(2,1)}, u32[]{:S(2)}) copy-start(bf16[128,128]{1,0:T(8,128)(2,1)} %param.20) | copy-start | bytes 98308
  0.7 5.8 %copy-start.6 = (bf16[128,512]{1,0:T(8,128)(2,1)S(1)}, bf16[128,512]{1,0:T(8,128)(2,1)}, u32[]{:S(2)}) copy-start(bf16[128,512]{1,0:T(8,128)(2,1)} %param.26) | copy-start | bytes 393220
  6.7 47.7 %copy-start.11 = (bf16[512]{0:T(512)(128)(2,1)S(1)}, bf16[512]{0:T(512)(128)(2,1)}, u32[]{:S(2)}) copy-start(bf16[512]{0:T(512)(128)(2,1)} %param.35) | copy-start | bytes 3076
  6.7 49.7 %copy-start.13 = (s32[4]{0:T(128)S(1)}, s32[4]{0:T(128)}, u32[]{:S(2)}) copy-start(s32[4]{0:T(128)} %param.21) | copy-start | bytes 52
  6.7 49.7 %copy-start.14 = (f32[8]{0:T(128)S(1)}, f32[8]{0:T(128)}, u32[]{:S(2)}) copy-start(f32[8]{0:T(128)} %param.32) | copy-start | bytes 100
  6.7 49.7 %copy-start.10 = (bf16[4,2,128]{2,1,0:T(2,128)(2,1)S(1)}, bf16[4,2,128]{2,1,0:T(2,128)(2,1)}, u32[]{:S(2)}) copy-start(bf16[4,2,128]{2,1,0:T(2,128)(2,1)} %param.34) | copy-start | bytes 6148
  6.7 49.7 %copy-start.7 = (bf16[4,512]{1,0:T(4,128)(2,1)S(1)}, bf16[4,512]{1,0:T(4,128)(2,1)}, u32[]{:S(2)}) copy-start(bf16[4,512]{1,0:T(4,128)(2,1)} %param.33) | copy-start | bytes 12292
  7.9 48.5 %copy-start.9 = (bf16[4,3,2,128]{3,2,1,0:T(2,128)(2,1)S(1)}, bf16[4,3,2,128]{3,2,1,0:T(2,128)(2,1)}, u32[]{:S(2)}) copy-start(bf16[4,3,2,128]{3,2,1,0:T(2,128)(2,1)} %param.23) | copy-start | bytes 18436
  7.9 48.6 %copy-start.8 = (bf16[4,3,512]{2,0,1:T(4,128)(2,1)S(1)}, bf16[4,3,512]{2,0,1:T(4,128)(2,1)}, u32[]{:S(2)}) copy-start(bf16[4,3,512]{2,0,1:T(4,128)(2,1)} %param.22) | copy-start | bytes 36868
  8.0 128.2 %copy-start.12 = (f32[8]{0:T(128)S(1)}, f32[8]{0:T(128)}, u32[]{:S(2)}) copy-start(f32[8]{0:T(128)} %param.31) | copy-start | bytes 100
  8.0 128.4 %copy-start.3 = (f32[4,8,64,128]{3,2,1,0:T(8,128)S(1)}, f32[4,8,64,128]{3,2,1,0:T(8,128)}, u32[]{:S(2)}) copy-start(f32[4,8,64,128]{3,2,1,0:T(8,128)} %param.24) | copy-start | bytes 3145732
  8.0 127.6 %all-to-all-start = ((f32[32,4,1289]{2,1,0:T(4,128)}), f32[32,4,1289]{2,1,0:T(4,128)S(1)}, u32[]{:S(2)}, u32[]{:S(2)}) async-start(f32[32,4,1289]{2,1,0:T(4,128)} %concatenate.30), calls=%async_computation | async-start | bytes 1441792 | tf_op jit(solution)/shard_map/all_to_all | solution.py:21
  136.8 102.2 %copy-start.1 = (f32[4,8,64,128]{3,2,1,0:T(8,128)}, f32[4,8,64,128]{3,2,1,0:T(8,128)S(1)}, u32[]{:S(2)}) copy-start(f32[4,8,64,128]{3,2,1,0:T(8,128)S(1)} %multiply_add_fusion) | copy-start | bytes 3145732
  136.8 101.2 %copy-start.5 = (bf16[512,128]{1,0:T(8,128)(2,1)S(1)}, bf16[512,128]{1,0:T(8,128)(2,1)}, u32[]{:S(2)}) copy-start(bf16[512,128]{1,0:T(8,128)(2,1)} %param.36) | copy-start | bytes 393220
  179.1 59.1 %all-to-all-start.2 = ((f32[8,1,128]{2,1,0:T(1,128)}), f32[8,1,128]{2,1,0:T(1,128)S(1)}, u32[]{:S(2)}, u32[]{:S(2)}) async-start(f32[8,1,128]{2,1,0:T(1,128)} %broadcast_in_dim.9), calls=%async_computation.2 | async-start | bytes 8192 | tf_op jit(solution)/shard_map/all_to_all | solution.py:38
  237.9 19.6 %copy-start.15 = (bf16[128]{0:T(256)(128)(2,1)S(1)}, bf16[128]{0:T(256)(128)(2,1)}, u32[]{:S(2)}) copy-start(bf16[128]{0:T(256)(128)(2,1)} %param.37) | copy-start | bytes 772
  239.0 27.9 %all-to-all-start.1 = ((f32[8,128,128]{2,1,0:T(8,128)}), f32[8,128,128]{2,1,0:T(8,128)S(1)}, u32[]{:S(2)}, u32[]{:S(2)}) async-start(f32[8,128,128]{2,1,0:T(8,128)} %broadcast_in_dim.8), calls=%async_computation.1 | async-start | bytes 1048576 | tf_op jit(solution)/shard_map/all_to_all | solution.py:38
  389.0 64.9 %copy-start.4 = (bf16[2048,128]{1,0:T(8,128)(2,1)S(1)}, bf16[2048,128]{1,0:T(8,128)(2,1)}, u32[]{:S(2)}) copy-start(bf16[2048,128]{1,0:T(8,128)(2,1)} %param.39) | copy-start | bytes 1572868
where the time goes:
time: 472 us; the launch traced here: 471 us
  blocking collectives  281 us (60%)
  waiting for transfers between devices  88.3 us (19%)
  starting transfers between devices  83.6 us (18%)
  matrix products  6.45 us (1%)
  local copies, waits for them, and re-layouts  5.78 us (1%)
    all_to_all x1, blocking collectives, summed_on_arrival(): lax.all_to_all(parts, axis, split_axis=0, concat_axis=0, tiled=True)  120 us
    all_to_all x2, blocking collectives, from_everyone(): return lax.all_to_all(copies, axis, split_axis=0, concat_axis=0, tiled=True)  81.3 us
    all_to_all x1, waiting for transfers between devices, summed_on_arrival(): lax.all_to_all(parts, axis, split_axis=0, concat_axis=0, tiled=True)  79 us
    all_to_all x1, starting transfers between devices, summed_on_arrival(): lax.all_to_all(parts, axis, split_axis=0, concat_axis=0, tiled=True)  46.4 us
    all_gather x1, blocking collectives, per_device(): lax.all_gather(gated_low, 'kv', axis=0, tiled=True)  40.2 us
    unnamed x1, blocking collectives  39.4 us
    all_to_all x2, starting transfers between devices, from_everyone(): return lax.all_to_all(copies, axis, split_axis=0, concat_axis=0, tiled=True)  37.2 us
  transfers between devices with their start and end apart: 3, of which 2 were waited for; matrix products, arithmetic and copies ran while one was open for 0% of the time, Pallas kernels for 0%

commit v1 on v0

--- a/solution.py
+++ b/solution.py
@@ -9,6 +9,11 @@
 CONV_WIDTH = 4
 INNER = 4096
 epsilon = 1e-06
+
+
+def read_row(dim_i, content):
+    current_block = jnp.concatenate(lax.psum(1, "kv") * [content], axis=dim_i)
+    return lax.all_to_all(current_block, "kv", dim_i, dim_i, tiled=True)
 
 
 def in_blocks(shard, dim, size):
@@ -136,7 +141,7 @@
     gated_rows = mixer_y * jax.nn.silu(gate_raw * inverse)
     gated_low = (gated_rows * inner_gain.astype(jnp.float32)).astype(jnp.bfloat16)
     all_low, all_squares = (
-        lax.all_gather(gated_low, "kv", axis=0, tiled=True),
+        read_row(0, gated_low),
         lax.all_gather(
             jnp.sum(gated_rows * gated_rows, axis=1).astype(jnp.bfloat16), "kv", axis=0, tiled=True
         ).astype(jnp.float32),

time: 472 us -> 452 us (0.958)
  blocking collectives: 281 us -> 263 us
  starting transfers between devices: 83.6 us -> 73.2 us
  waiting for transfers between devices: 88.3 us -> 94.5 us
    all_gather x1 -> x0, blocking collectives: 40.2 us -> none  [per_device(): lax.all_gather(gated_low, 'kv', axis=0, tiled=True)]
    all_to_all x2, starting transfers between devices: 37.2 us -> 22 us  [from_everyone(): return lax.all_to_all(copies, axis, split_axis=0, concat_axis=0, tiled=True)]
    all_to_all x1, blocking collectives: 120 us -> 133 us  [summed_on_arrival(): lax.all_to_all(parts, axis, split_axis=0, concat_axis=0, tiled=True)]
    unnamed x1, blocking collectives: 39.4 us -> 48.8 us
    all_to_all x0 -> x1, starting transfers between devices: none -> 4.77 us  [read_row(): return lax.all_to_all(current_block, 'kv', dim_i, dim_i, tiled=True)]
  transfers between devices with their start and end apart: 3 -> 4, of which waited for: 2 -> 3; matrix products, arithmetic and copies ran while one was open for 0% -> 0% of each run, Pallas kernels for 0% -> 0%
where the time goes in v1:
time: 452 us; the launch traced here: 451 us
  blocking collectives  263 us (58%)
  waiting for transfers between devices  94.5 us (21%)
  starting transfers between devices  73.2 us (16%)
  local copies, waits for them, and re-layouts  7.02 us (2%)
  matrix products  6.45 us (1%)
  other arithmetic  4.55 us (1%)
    all_to_all x1, blocking collectives, summed_on_arrival(): lax.all_to_all(parts, axis, split_axis=0, concat_axis=0, tiled=True)  133 us
    all_to_all x2, blocking collectives, from_everyone(): return lax.all_to_all(copies, axis, split_axis=0, concat_axis=0, tiled=True)  81.3 us
    all_to_all x1, waiting for transfers between devices, summed_on_arrival(): lax.all_to_all(parts, axis, split_axis=0, concat_axis=0, tiled=True)  80.8 us
    unnamed x1, blocking collectives  48.8 us
    all_to_all x1, starting transfers between devices, summed_on_arrival(): lax.all_to_all(parts, axis, split_axis=0, concat_axis=0, tiled=True)  46.4 us
    all_to_all x2, starting transfers between devices, from_everyone(): return lax.all_to_all(copies, axis, split_axis=0, concat_axis=0, tiled=True)  22 us
    all_to_all x2, waiting for transfers between devices, from_everyone(): return lax.all_to_all(copies, axis, split_axis=0, concat_axis=0, tiled=True)  13.7 us
  transfers between devices with their start and end apart: 4, of which 3 were waited for; matrix products, arithmetic and copies ran while one was open for 0% of the time, Pallas kernels for 0%

profile of v1, /device:TPU:33, one launch (start us, length us, event | category | flops | bytes accessed | tf_op | source)
XLA Modules:
  0.0 450.8 jit_solution(11315961585116401028)
XLA Ops:
  0.7 0.7 convert_element_type.73
  1.4 0.9 fusion.1
  2.3 0.3 concatenate.38
  2.5 0.9 fusion.16
  3.4 0.9 fusion.14
  4.3 0.9 fusion.12
  5.2 1.1 fusion.18
  6.4 0.2 fusion.20
  6.8 1.2 concatenate.33
  8.0 46.4 %all-to-all-start = ((f32[32,4,1289]{2,1,0:T(4,128)}), f32[32,4,1289]{2,1,0:T(4,128)S(1)}, u32[]{:S(2)}, u32[]{:S(2)}) async-start(f32[32,4,1289]{2,1,0:T(4,128)} %concatenate.33), calls=%async_computation | async-start | bytes 1441792 | tf_op jit(solution)/shard_map/all_to_all | solution.py:26
  54.4 0.1 copy.45
  54.8 80.8 %all-to-all-done = f32[32,4,1289]{2,1,0:T(4,128)S(1)} async-done(((f32[32,4,1289]{2,1,0:T(4,128)}), f32[32,4,1289]{2,1,0:T(4,128)S(1)}, u32[]{:S(2)}, u32[]{:S(2)}) %all-to-all-start) | async-done | bytes 660000 | tf_op jit(solution)/shard_map/all_to_all | solution.py:26
  135.6 0.1 reduce_sum.73
  135.7 0.2 fusion.41
  136.0 0.1 divide_multiply_fusion.1
  136.2 0.1 multiply_exponential_fusion
  136.4 0.4 multiply_add_fusion
  136.8 1.7 fusion.47
  138.5 0.1 reshape.102
  138.6 0.2 multiply_reduce_fusion
  138.8 0.5 concatenate.34
  139.3 0.7 all_to_all.28
  140.0 4.8 %all-to-all-start.1 = ((bf16[32,4,512]{2,1,0:T(4,128)(2,1)}), bf16[32,4,512]{2,1,0:T(4,128)(2,1)S(1)}, u32[]{:S(2)}, u32[]{:S(2)}) async-start(bf16[32,4,512]{2,1,0:T(4,128)(2,1)} %all_to_all.28), calls=%async_computation.1 | async-start | bytes 262144 | tf_op jit(solution)/shard_map/all_to_all | solution.py:16
  144.8 1.3 dynamic-slice
  146.7 0.2 dynamic-update-slice
  146.9 48.8 %all-reduce = bf16[128]{0:T(256)(128)(2,1)S(1)} all-reduce(bf16[128]{0:T(256)(128)(2,1)S(1)} %dynamic-update-slice), channel_id=1, replica_groups=mesh['grp'=2,'kv'=32,'tp'=8] {'kv'}, use_global_device_ids=true, to_apply=%add | all-reduce | flops 128 | bytes 512
  195.8 0.6 broadcast_in_dim.9
  196.3 17.9 %all-to-all-start.3 = ((f32[8,1,128]{2,1,0:T(1,128)}), f32[8,1,128]{2,1,0:T(1,128)S(1)}, u32[]{:S(2)}, u32[]{:S(2)}) async-start(f32[8,1,128]{2,1,0:T(1,128)} %broadcast_in_dim.9), calls=%async_computation.3 | async-start | bytes 8192 | tf_op jit(solution)/shard_map/all_to_all | solution.py:43
  214.3 0.2 fusion.48
  214.5 4.3 all-to-all-done.3
  218.8 0.8 broadcast_in_dim.8
  219.6 4.1 all-to-all-start.2
  223.7 9.4 %all-to-all-done.2 = f32[8,128,128]{2,1,0:T(8,128)S(1)} async-done(((f32[8,128,128]{2,1,0:T(8,128)}), f32[8,128,128]{2,1,0:T(8,128)S(1)}, u32[]{:S(2)}, u32[]{:S(2)}) %all-to-all-start.2) | async-done | bytes 524320 | tf_op jit(solution)/shard_map/all_to_all | solution.py:43
  233.2 0.2 fusion.4
  233.3 0.3 concatenate.39
  233.6 0.3 fusion.6
  233.9 0.3 concatenate.35
  234.2 0.2 pad_maximum_fusion
  234.5 133.3 %all_to_all.43 = f32[32,4,2049]{2,1,0:T(4,128)S(1)} all-to-all(f32[32,4,2049]{2,1,0:T(4,128)S(1)} %pad_maximum_fusion), channel_id=1, replica_groups=mesh['grp'=2,'kv'=32,'tp'=8] {'kv'}, dimensions={0} | all-to-all | bytes 2098176 | tf_op jit(solution)/shard_map/all_to_all | solution.py:26
  367.7 0.2 reduce_sum.78
  367.9 0.1 fusion.38
  368.0 0.1 fusion.10
  368.1 0.2 broadcast_in_dim.10
  368.4 64.8 %all_to_all.44 = bf16[32,4,2048]{2,1,0:T(4,128)(2,1)S(1)} all-to-all(bf16[32,4,2048]{2,1,0:T(4,128)(2,1)S(1)} %broadcast_in_dim.10), channel_id=1, replica_groups=mesh['grp'=2,'kv'=32,'tp'=8] {'kv'}, dimensions={0} | all-to-all | bytes 1048576 | tf_op jit(solution)/shard_map/all_to_all | solution.py:43
  433.2 0.1 reshape.103
  433.3 0.3 fusion.49
  433.6 16.5 %all_to_all.45 = f32[8,128,128]{2,1,0:T(8,128)S(1)} all-to-all(f32[8,128,128]{2,1,0:T(8,128)S(1)} %broadcast_in_dim.11), channel_id=1, replica_groups=mesh['grp'=2,'kv'=32,'tp'=8] {'tp'}, dimensions={0} | all-to-all | bytes 1048576 | tf_op jit(solution)/shard_map/all_to_all | solution.py:43
  450.1 0.6 fusion.5
  (58 shorter events, 0.9 us)
Async XLA Ops:
  0.6 233.0 %copy-start = (bf16[128,2048]{1,0:T(8,128)(2,1)S(1)}, bf16[128,2048]{1,0:T(8,128)(2,1)}, u32[]{:S(2)}) copy-start(bf16[128,2048]{1,0:T(8,128)(2,1)} %param.38) | copy-start | bytes 1572868
  0.6 5.8 %copy-start.2 = (bf16[128,128]{1,0:T(8,128)(2,1)S(1)}, bf16[128,128]{1,0:T(8,128)(2,1)}, u32[]{:S(2)}) copy-start(bf16[128,128]{1,0:T(8,128)(2,1)} %param.20) | copy-start | bytes 98308
  0.7 5.8 %copy-start.6 = (bf16[128,512]{1,0:T(8,128)(2,1)S(1)}, bf16[128,512]{1,0:T(8,128)(2,1)}, u32[]{:S(2)}) copy-start(bf16[128,512]{1,0:T(8,128)(2,1)} %param.26) | copy-start | bytes 393220
  6.7 47.7 %copy-start.13 = (s32[4]{0:T(128)S(1)}, s32[4]{0:T(128)}, u32[]{:S(2)}) copy-start(s32[4]{0:T(128)} %param.21) | copy-start | bytes 52
  6.7 47.8 %copy-start.11 = (bf16[512]{0:T(512)(128)(2,1)S(1)}, bf16[512]{0:T(512)(128)(2,1)}, u32[]{:S(2)}) copy-start(bf16[512]{0:T(512)(128)(2,1)} %param.35) | copy-start | bytes 3076
  6.7 47.8 %copy-start.14 = (f32[8]{0:T(128)S(1)}, f32[8]{0:T(128)}, u32[]{:S(2)}) copy-start(f32[8]{0:T(128)} %param.32) | copy-start | bytes 100
  6.7 47.8 %copy-start.10 = (bf16[4,2,128]{2,1,0:T(2,128)(2,1)S(1)}, bf16[4,2,128]{2,1,0:T(2,128)(2,1)}, u32[]{:S(2)}) copy-start(bf16[4,2,128]{2,1,0:T(2,128)(2,1)} %param.34) | copy-start | bytes 6148
  6.7 47.8 %copy-start.7 = (bf16[4,512]{1,0:T(4,128)(2,1)S(1)}, bf16[4,512]{1,0:T(4,128)(2,1)}, u32[]{:S(2)}) copy-start(bf16[4,512]{1,0:T(4,128)(2,1)} %param.33) | copy-start | bytes 12292
  7.9 46.7 %copy-start.9 = (bf16[4,3,2,128]{3,2,1,0:T(2,128)(2,1)S(1)}, bf16[4,3,2,128]{3,2,1,0:T(2,128)(2,1)}, u32[]{:S(2)}) copy-start(bf16[4,3,2,128]{3,2,1,0:T(2,128)(2,1)} %param.23) | copy-start | bytes 18436
  7.9 46.7 %copy-start.8 = (bf16[4,3,512]{2,0,1:T(4,128)(2,1)S(1)}, bf16[4,3,512]{2,0,1:T(4,128)(2,1)}, u32[]{:S(2)}) copy-start(bf16[4,3,512]{2,0,1:T(4,128)(2,1)} %param.22) | copy-start | bytes 36868
  8.0 128.2 %copy-start.12 = (f32[8]{0:T(128)S(1)}, f32[8]{0:T(128)}, u32[]{:S(2)}) copy-start(f32[8]{0:T(128)} %param.31) | copy-start | bytes 100
  8.0 128.4 %copy-start.3 = (f32[4,8,64,128]{3,2,1,0:T(8,128)S(1)}, f32[4,8,64,128]{3,2,1,0:T(8,128)}, u32[]{:S(2)}) copy-start(f32[4,8,64,128]{3,2,1,0:T(8,128)} %param.24) | copy-start | bytes 3145732
  8.0 127.6 %all-to-all-start = ((f32[32,4,1289]{2,1,0:T(4,128)}), f32[32,4,1289]{2,1,0:T(4,128)S(1)}, u32[]{:S(2)}, u32[]{:S(2)}) async-start(f32[32,4,1289]{2,1,0:T(4,128)} %concatenate.33), calls=%async_computation | async-start | bytes 1441792 | tf_op jit(solution)/shard_map/all_to_all | solution.py:26
  136.8 77.5 %copy-start.1 = (f32[4,8,64,128]{3,2,1,0:T(8,128)}, f32[4,8,64,128]{3,2,1,0:T(8,128)S(1)}, u32[]{:S(2)}) copy-start(f32[4,8,64,128]{3,2,1,0:T(8,128)S(1)} %multiply_add_fusion) | copy-start | bytes 3145732
  136.8 77.5 %copy-start.5 = (bf16[512,128]{1,0:T(8,128)(2,1)S(1)}, bf16[512,128]{1,0:T(8,128)(2,1)}, u32[]{:S(2)}) copy-start(bf16[512,128]{1,0:T(8,128)(2,1)} %param.36) | copy-start | bytes 393220
  140.0 55.8 %all-to-all-start.1 = ((bf16[32,4,512]{2,1,0:T(4,128)(2,1)}), bf16[32,4,512]{2,1,0:T(4,128)(2,1)S(1)}, u32[]{:S(2)}, u32[]{:S(2)}) async-start(bf16[32,4,512]{2,1,0:T(4,128)(2,1)} %all_to_all.28), calls=%async_computation.1 | async-start | bytes 262144 | tf_op jit(solution)/shard_map/all_to_all | solution.py:16
  196.3 22.4 %all-to-all-start.3 = ((f32[8,1,128]{2,1,0:T(1,128)}), f32[8,1,128]{2,1,0:T(1,128)S(1)}, u32[]{:S(2)}, u32[]{:S(2)}) async-start(f32[8,1,128]{2,1,0:T(1,128)} %broadcast_in_dim.9), calls=%async_computation.3 | async-start | bytes 8192 | tf_op jit(solution)/shard_map/all_to_all | solution.py:43
  214.2 9.5 %copy-start.15 = (bf16[128]{0:T(256)(128)(2,1)S(1)}, bf16[128]{0:T(256)(128)(2,1)}, u32[]{:S(2)}) copy-start(bf16[128]{0:T(256)(128)(2,1)} %param.37) | copy-start | bytes 772
  219.6 13.5 %all-to-all-start.2 = ((f32[8,128,128]{2,1,0:T(8,128)}), f32[8,128,128]{2,1,0:T(8,128)S(1)}, u32[]{:S(2)}, u32[]{:S(2)}) async-start(f32[8,128,128]{2,1,0:T(8,128)} %broadcast_in_dim.8), calls=%async_computation.2 | async-start | bytes 1048576 | tf_op jit(solution)/shard_map/all_to_all | solution.py:43
  368.3 65.0 %copy-start.4 = (bf16[2048,128]{1,0:T(8,128)(2,1)S(1)}, bf16[2048,128]{1,0:T(8,128)(2,1)}, u32[]{:S(2)}) copy-start(bf16[2048,128]{1,0:T(8,128)(2,1)} %param.39) | copy-start | bytes 1572868
